TPU v7x, 128 devices: a whole 4x4x4 slice. The times are simulated.
128 devices in a mesh: sp: 16 (over z, y), tp: 8 (over x, core).
Axes of the slice: x: 4, y: 4, z: 4, core: 2. Of those that a mesh axis runs over, the one named last changes fastest.
Arguments:
- arriving_hidden_sum: bfloat16 [16384, 2048], P('sp'), may hold values from -40 to 40
- content_entries_clustered: bfloat16 [16384, 4096], P('sp', 'tp'), may hold values from -6 to 6
- leaving_switch_entries: bfloat16 [16384, 4096], P('sp', 'tp'), may hold values from -6 to 6
- linked_source_target_pairs: bfloat16 [16384, 8, 2, 128], P('sp', 'tp'), may hold values from -1.78125 to 1.78125
- raw_interval_length: bfloat16 [16384, 64], P('sp', 'tp'), may hold values from -5 to 5
- spike_extra_lognoise: float32 [16384, 64], P('sp', 'tp'), may hold values from -0.6 to 0
- content_filter_kernel: bfloat16 [4, 4096], P(None, 'tp'), may hold values from -3 to 3
- coupling_filter_kernel: bfloat16 [4, 8, 2, 128], P(None, 'tp'), may hold values from -3 to 3
- interval_shift_vector: float32 [64], P('tp'), may hold values from -0.5 to 0.5
- fading_speed_exponent: float32 [64], P('tp'), may hold values from -16 to -2.9
- skip_channel_factor: float32 [64], P('tp'), may hold values from 1 to 10
- cluster_rescale_vector: float32 [4096], P('tp'), may hold values from 0.1 to 1.9
- blender_final_tensor: bfloat16 [4096, 2048], P('tp'), may hold values from -0.09375 to 0.09375
- prelayer_rescale_vector: float32 [2048], replicated, may hold values from 0.1 to 1.9
- switching_linear_tensor: bfloat16 [2048, 5632], P('sp', 'tp'), may hold values from -0.125 to 0.125
- widening_linear_tensor: bfloat16 [2048, 5632], P('sp', 'tp'), may hold values from -0.125 to 0.125
- contracting_linear_tensor: bfloat16 [5632, 2048], P('tp', 'sp'), may hold values from -0.078125 to 0.078125
Outputs:
- residual_out: bfloat16 [16384, 2048], P('sp', 'tp')
All inputs are finite; a program needn't handle non-finite values.
Results may differ from a plain program's by a relative error of at most 0.012.
Values may be sent and summed in bfloat16 or wider, within the bound.
No kernel may reach another device: no remote copies, remote signals or barrier semaphores. Data moves between devices by JAX's collectives and lax.ppermute only.
A program may use at most 128 MiB of HBM per device.

v0:
```python
import jax
import jax.numpy as jnp
from jax import lax
from jax.sharding import Mesh
from jax.sharding import PartitionSpec as P

D = 2048
BLOCK_POSITIONS = 128
SP = ("sp_0", "sp_1")
EPS = 1e-06


def rows_first(arrays, axis, dims):
    turned = [jnp.moveaxis(a, dim, 0) for a, dim in zip(arrays, dims)]
    both = jnp.concatenate([t.reshape(len(t), -1) for t in turned], axis=1)
    out, at, outs = (lax.all_gather(both, axis, axis=0, tiled=True), 0, [])
    for t, dim in zip(turned, dims):
        piece = out[:, at : at + t[0].size].reshape(-1, *t.shape[1:])
        outs.append(jnp.moveaxis(piece, 0, dim))
        at += t[0].size
    return tuple(outs)


def from_behind(block, axis, distance):
    devices = range(lax.axis_size(axis))
    route = [(i - distance, i) for i in devices if i - distance in devices]
    return lax.ppermute(block, axis, route)


def neutral_like(array, identity):
    return jax.tree.map(
        lambda part, zero: jnp.zeros_like(part) + jnp.asarray(zero, part.dtype), array, identity
    )


def entering_2(array, axes, combine, identity):
    before = start = neutral_like(array, identity)
    so_far = array
    for axis in reversed(axes):
        count, place = (lax.axis_size(axis), lax.axis_index(axis))
        pieces = jax.tree.map(
            lambda part, kind: lax.all_gather(part.astype(kind), axis),
            so_far,
            (jnp.bfloat16, jnp.bfloat16),
        )
        inside, so_far = (start, start)
        for k in range(count):
            passed = k < place
            so_far = combine(
                so_far, jax.tree.map(lambda part, own: part[k].astype(own.dtype), pieces, array)
            )
            inside = jax.tree.map(lambda new, old: jnp.where(passed, new, old), so_far, inside)
        before = combine(inside, before)
    return before


def conv_block(values, rims, taps):
    taps_count = taps.shape[0]
    length = values.shape[0]
    padded = jnp.concatenate([rims, values], axis=0).astype(jnp.float32)
    running = jnp.zeros(values.shape, jnp.float32)
    for tap_index in range(taps_count):
        running = running + padded[tap_index : tap_index + length] * taps[tap_index].astype(
            jnp.float32
        )
    return jax.nn.silu(running).astype(jnp.bfloat16)


def combine_states(former, latter):
    return (former[0] * jnp.exp(latter[1])[:, :, None, None] + latter[0], former[1] + latter[1])


def shards(
    arriving_hidden_sum,
    content_entries_clustered,
    leaving_switch_entries,
    linked_source_target_pairs,
    raw_interval_length,
    spike_extra_lognoise,
    content_filter_kernel,
    coupling_filter_kernel,
    interval_shift_vector,
    fading_speed_exponent,
    skip_channel_factor,
    cluster_rescale_vector,
    blender_final_tensor,
    prelayer_rescale_vector,
    switching_linear_tensor,
    widening_linear_tensor,
    contracting_linear_tensor,
):
    whole_gate, whole_up, whole_down = rows_first(
        (switching_linear_tensor, widening_linear_tensor, contracting_linear_tensor), SP, (0, 0, 1)
    )
    length = content_entries_clustered.shape[0]
    heads_per_device = raw_interval_length.shape[1]
    groups_dev = linked_source_target_pairs.shape[1]
    per_group = heads_per_device // groups_dev
    head_size = content_entries_clustered.shape[1] // heads_per_device
    state_size = linked_source_target_pairs.shape[3]
    taps_count = content_filter_kernel.shape[0]
    block_count = length // BLOCK_POSITIONS
    couple_flat = linked_source_target_pairs.reshape(length, -1)
    value_rims, couple_rims = from_behind(
        (
            content_entries_clustered[length - taps_count + 1 :],
            couple_flat[length - taps_count + 1 :],
        ),
        SP,
        1,
    )
    values = conv_block(content_entries_clustered, value_rims, content_filter_kernel)
    coupled = conv_block(
        couple_flat, couple_rims, coupling_filter_kernel.reshape(taps_count, -1)
    ).reshape(length, groups_dev, 2, state_size)
    value_blocks = values.reshape(block_count, BLOCK_POSITIONS, heads_per_device, head_size)
    write_maps = coupled[:, :, 0].reshape(block_count, BLOCK_POSITIONS, groups_dev, state_size)
    read_maps = coupled[:, :, 1].reshape(block_count, BLOCK_POSITIONS, groups_dev, state_size)
    interval_lengths = jax.nn.softplus(
        raw_interval_length.astype(jnp.float32) + interval_shift_vector
    )
    fading_log_factor = (
        -jnp.exp(fading_speed_exponent) * interval_lengths + spike_extra_lognoise
    ).reshape(block_count, BLOCK_POSITIONS, heads_per_device)
    interval_lengths = interval_lengths.reshape(block_count, BLOCK_POSITIONS, heads_per_device)
    cum_log = jnp.cumsum(fading_log_factor, axis=1)
    head_cum = jnp.swapaxes(cum_log, 1, 2)
    log_gap = head_cum[:, :, :, None] - head_cum[:, :, None, :]
    causal = jnp.tril(jnp.ones((BLOCK_POSITIONS, BLOCK_POSITIONS), bool))
    intersection = jnp.einsum(
        "blgn,bsgn->bgls", read_maps, write_maps, preferred_element_type=jnp.float32
    )
    intersection = jnp.repeat(intersection, per_group, axis=1)
    weights = (
        intersection
        * jnp.exp(jnp.where(causal, log_gap, -jnp.inf))
        * jnp.swapaxes(interval_lengths, 1, 2)[:, :, None, :]
    ).astype(jnp.bfloat16)
    within = jnp.einsum(
        "bhls,bshp->blhp", weights, value_blocks, preferred_element_type=jnp.float32
    )
    end_log = cum_log[:, -1]
    scaled = (
        value_blocks * (interval_lengths * jnp.exp(end_log[:, None, :] - cum_log))[..., None]
    ).astype(jnp.bfloat16)
    block_states = jnp.einsum(
        "blgn,blgrp->bgrpn",
        write_maps,
        scaled.reshape(block_count, BLOCK_POSITIONS, groups_dev, per_group, head_size),
        preferred_element_type=jnp.float32,
    )
    end_grouped = end_log.reshape(block_count, groups_dev, per_group)

    def carry_step(carry_state, inputs):
        block_added, block_end = inputs
        return (carry_state * jnp.exp(block_end)[:, :, None, None] + block_added, carry_state)

    zeros_state = jnp.zeros((groups_dev, per_group, head_size, state_size), jnp.float32)
    final_state, entering = lax.scan(carry_step, zeros_state, (block_states, end_grouped))
    read_wide = read_maps.astype(jnp.float32)
    carried = (
        jnp.einsum("blgn,bgrpn->blgrp", read_wide, entering).reshape(
            block_count, BLOCK_POSITIONS, heads_per_device, head_size
        )
        * jnp.exp(cum_log)[..., None]
    )
    device_log = jnp.sum(end_log, axis=0).reshape(groups_dev, per_group)
    incoming, _ = entering_2(
        (final_state, device_log), SP, combine_states, (zeros_state, jnp.zeros_like(device_log))
    )
    prior_log = jnp.cumsum(end_log, axis=0) - end_log
    reach_decay = jnp.exp(cum_log + prior_log[:, None, :])
    arrived = (
        jnp.einsum("blgn,grpn->blgrp", read_wide, incoming).reshape(
            block_count, BLOCK_POSITIONS, heads_per_device, head_size
        )
        * reach_decay[..., None]
    )
    mixer = (within + carried + arrived).reshape(
        length, heads_per_device, head_size
    ) + values.reshape(length, heads_per_device, head_size).astype(
        jnp.float32
    ) * skip_channel_factor[
        None, :, None
    ]
    gated = mixer.reshape(length, heads_per_device * head_size) * jax.nn.silu(
        leaving_switch_entries.astype(jnp.float32)
    )
    grouped = gated.reshape(length, groups_dev, per_group * head_size)
    grouped = grouped * lax.rsqrt(jnp.mean(grouped * grouped, axis=-1, keepdims=True) + EPS)
    mixed_rows = (
        grouped.reshape(length, heads_per_device * head_size) * cluster_rescale_vector
    ).astype(jnp.bfloat16)
    partial_sum = jnp.dot(mixed_rows, blender_final_tensor, preferred_element_type=jnp.float32)
    rounded = lax.optimization_barrier(partial_sum.astype(jnp.bfloat16)).astype(jnp.float32)
    col_count = D // lax.axis_size("tp")
    offset = lax.axis_index("tp") * col_count
    mixer_out = lax.psum(rounded.astype(jnp.bfloat16), "tp").astype(jnp.float32)
    residual_whole = (arriving_hidden_sum.astype(jnp.float32) + mixer_out).astype(jnp.bfloat16)
    squares = residual_whole.astype(jnp.float32)
    normed = (
        squares
        * lax.rsqrt(jnp.mean(squares * squares, axis=-1, keepdims=True) + EPS)
        * prelayer_rescale_vector
    ).astype(jnp.bfloat16)
    residual_mid = lax.dynamic_slice_in_dim(residual_whole, offset, col_count, 1)
    gate_pre = jnp.dot(normed, whole_gate, preferred_element_type=jnp.float32)
    up_pre = jnp.dot(normed, whole_up, preferred_element_type=jnp.float32)
    hidden = (jax.nn.silu(gate_pre) * up_pre).astype(jnp.bfloat16)
    down_terms = jnp.dot(hidden, whole_down, preferred_element_type=jnp.float32)
    down_rounded = lax.optimization_barrier(down_terms.astype(jnp.bfloat16)).astype(jnp.float32)
    mlp_cols = lax.psum_scatter(
        down_rounded.astype(jnp.bfloat16), "tp", scatter_dimension=1, tiled=True
    ).astype(jnp.float32)
    return (residual_mid.astype(jnp.float32) + 0.5 * mlp_cols).astype(jnp.bfloat16)


def solution(mesh):
    torus = Mesh(mesh.devices.reshape(4, 4, mesh.shape["tp"]), ("sp_0", "sp_1", "tp"))
    return jax.shard_map(
        shards,
        mesh=torus,
        in_specs=(
            P(SP, None),
            P(SP, "tp"),
            P(SP, "tp"),
            P(SP, "tp", None, None),
            P(SP, "tp"),
            P(SP, "tp"),
            P(None, "tp"),
            P(None, "tp", None, None),
            P("tp"),
            P("tp"),
            P("tp"),
            P("tp"),
            P("tp", None),
            P(),
            P(SP, "tp"),
            P(SP, "tp"),
            P("tp", SP),
        ),
        out_specs=P(SP, "tp"),
        check_vma=False,
    )
```

profile of v0, /device:TPU:0, one launch (start us, length us, event | category | flops | bytes accessed | tf_op | source)
XLA Modules:
  0.0 283.2 jit_solution(7769426850520135814)
XLA Ops:
  7.4 0.8 slice.136
  9.0 4.2 %collective-permute-start.1 = (bf16[3,256]{0,1:T(8,128)(2,1)}, bf16[3,256]{0,1:T(8,128)(2,1)}, u32[]{:S(2)}, u32[]{:S(2)}) collective-permute-start(bf16[3,256]{0,1:T(8,128)(2,1)} %bitcast.4), channel_id=1, source_target_pairs={{0,8},{8,16},{16,24},{24,32},{32,40},{40,48},{48,56},{56,64},{64,7... | collective-permute-start | bytes 4616 | tf_op jit(solution)/shard_map/ppermute | solution.py:27
  14.7 2.9 %collective-permute-start = (bf16[3,512]{0,1:T(8,128)(2,1)}, bf16[3,512]{0,1:T(8,128)(2,1)S(1)}, u32[]{:S(2)}, u32[]{:S(2)}) collective-permute-start(bf16[3,512]{0,1:T(8,128)(2,1)} %copy.50), channel_id=1, source_target_pairs={{0,8},{8,16},{16,24},{24,32},{32,40},{40,48},{48,56},{56,64},{64,7... | collective-permute-start | bytes 9224 | tf_op jit(solution)/shard_map/ppermute | solution.py:27
  18.2 1.3 bitcast_convert_fusion.3
  19.5 0.8 slice_convert_fusion.3
  20.4 1.5 fusion.102
  22.1 1.0 copy.56
  23.1 1.2 fusion.107
  25.9 10.7 %all-reduce = bf16[32]{0:T(256)(128)(2,1)S(1)} all-reduce(bf16[32]{0:T(256)(128)(2,1)S(1)} %dynamic-update-slice), channel_id=2, replica_groups=mesh['sp_0'=4,'sp_1'=4,'tp'=8] {'sp_1'}, use_global_device_ids=true, to_apply=%add | all-reduce | flops 32 | bytes 128
  36.7 9.3 %all_gather.22 = bf16[4,1,8]{2,1,0:T(2,128)(2,1)S(1)} all-gather(bf16[1,1,8]{2,1,0:T(2,128)(2,1)S(1)} %get-tuple-element.82), channel_id=1, replica_groups=mesh['sp_0'=4,'sp_1'=4,'tp'=8] {'sp_0'}, dimensions={0}, use_global_device_ids=true | all-gather | bytes 80 | tf_op jit(solution)/shard_map/all_gather | solution.py:42
  46.5 1.3 fusion.105
  49.1 2.0 copy.53
  51.1 2.3 copy.51
  54.9 1.5 copy.69
  56.4 1.8 copy.65
  58.2 1.8 copy.67
  60.0 1.8 copy.61
  61.8 1.3 maximum_convert_fusion.1
  63.1 1.8 multiply_convert_fusion.7
  65.8 1.8 copy.55
  67.6 1.8 copy.54
  69.4 2.1 fusion.108
  71.5 1.8 maximum_convert_fusion
  73.3 2.2 fusion.116
  76.5 1.8 convolution_bitcast_fusion
  78.3 19.0 %while.13 = (s32[]{:T(128)}, f32[1,8,64,128]{3,2,1,0:T(8,128)S(1)}, bf16[8,1,8,64,128]{4,3,2,1,0:T(8,128)(2,1)}, f32[8,1,8]{2,1,0:T(1,128)}, f32[8,1,8,64,128]{4,3,2,1,0:T(8,128)}, /*index=5*/s32[]{:T(128)}, s32[]{:T(128)}) while((s32[]{:T(128)}, f32[1,8,64,128]{3,2,1,0:T(8,128)S(1)}, bf16[8,1,8,64,128]{4,3,2,1,0:T(8,128)(2,1)}, ...), condition=%wide.region_2.3_spmd.clone, body=%wide.region_1.2_spmd.clone.sunk | while | flops 262147 | bytes 1179852 | solution.py:159
  79.7 1.0 bitcast_add_fusion.3
  82.0 1.0 bitcast_add_fusion.3
  84.3 1.0 bitcast_add_fusion.3
  86.7 1.0 bitcast_add_fusion.3
  89.1 1.0 bitcast_add_fusion.3
  91.5 1.0 bitcast_add_fusion.3
  93.9 1.0 bitcast_add_fusion.3
  96.2 1.0 bitcast_add_fusion.3
  97.3 12.9 %all-gather.1 = bf16[4,8,64,128]{3,2,1,0:T(8,128)(2,1)S(1)} all-gather(bf16[1,8,64,128]{3,2,1,0:T(8,128)(2,1)S(1)} %convert_element_type.347), channel_id=3, replica_groups=mesh['sp_0'=4,'sp_1'=4,'tp'=8] {'sp_1'}, dimensions={0}, use_global_device_ids=true | all-gather | bytes 655360 | tf_op jit(solution)/shard_map/all_gather | solution.py:42
  110.5 13.1 %all_gather.25 = bf16[4,1,8,64,128]{4,3,2,1,0:T(8,128)(2,1)S(1)} all-gather(bf16[1,1,8,64,128]{4,3,2,1,0:T(8,128)(2,1)S(1)} %fusion.66), channel_id=1, replica_groups=mesh['sp_0'=4,'sp_1'=4,'tp'=8] {'sp_0'}, dimensions={0}, use_global_device_ids=true | all-gather | bytes 655360 | tf_op jit(solution)/shard_map/all_gather | solution.py:42
  124.2 1.6 fusion.10
  126.8 1.2 copy.68
  128.4 2.9 %multiply_reduce_fusion = (f32[1024]{0:T(1024)S(1)}, f32[1024,512]{0,1:T(8,128)S(1)}) fusion(bf16[1024,512]{0,1:T(8,128)(2,1)S(1)} %copy.69, f32[512]{0:T(512)S(1)} %copy-done.20, f32[64,8,8,128]{3,2,1,0:T(8,128)S(1)} %bitcast.152, f32[512]{0:T(512)S(1)} %bitcast.169, f32[1027,512]{0,1:T(8,128)S(1)} %copy-done.3, f32[512]{0:T(512)S(1)} %bitcast.171, ...), kind=kLoop, calls=%fused_computation.42 | loop fusion | flops 12057600 | bytes 13645824 | tf_op jit(solution)/shard_map/reduce_sum | solution.py:190
  131.3 4.5 %convolution_convert_fusion.1 = bf16[1024,2048]{1,0:T(8,128)(2,1)} fusion(bf16[512,2048]{1,0:T(8,128)(2,1)S(1)} %copy-done, f32[1024,512]{0,1:T(8,128)S(1)} %get-tuple-element.81, f32[512]{0:T(512)S(1)} %copy-done.32, f32[1024]{0:T(1024)S(1)} %add_rsqrt_fusion.1), kind=kOutput, calls=%fused_computation.13 | convolution fusion | flops 2151153664 | bytes 8394752 | tf_op jit(solution)/shard_map/dot_general | solution.py:194
  135.9 0.8 copy-done.10
  136.9 0.8 pad_maximum_fusion
  138.1 69.1 %all-reduce.3.cloned.1.call-done = bf16[1024,2048]{1,0:T(8,128)(2,1)} async-done(((bf16[1024,2048]{1,0:T(8,128)(2,1)}), bf16[1024,2048]{1,0:T(8,128)(2,1)}) %all-reduce.3.cloned.1.call-update) | async-done | bytes 4194320 | tf_op jit(solution)/shard_map/psum | solution.py:198
  207.2 7.5 %fusion.2 = (f32[1024]{0:T(1024)S(1)}, bf16[1024,2048]{1,0:T(8,128)(2,1)}) fusion(bf16[1024,2048]{1,0:T(8,128)(2,1)} %all-reduce.3.cloned.1.call-done, bf16[1024,2048]{1,0:T(8,128)(2,1)} %param.19), kind=kLoop, calls=%fused_computation.7 | loop fusion | flops 14679040 | bytes 12587008 | tf_op jit(solution)/shard_map/reduce_sum | solution.py:203
  214.9 7.9 %fusion.8 = f32[1024,704]{0,1:T(8,128)} fusion(bf16[2048,2112]{0,1:T(8,128)(2,1)} %all-gather.4.cloned.1.call-done, bf16[1024,2048]{1,0:T(8,128)(2,1)} %get-tuple-element.79, f32[2048]{0:T(1024)S(1)} %copy-done.31, f32[1024]{0:T(1024)S(1)} %add_rsqrt_fusion), kind=kOutput, calls=%fused_computation.17 | convolution fusion | flops 2961178624 | bytes 9973760 | tf_op jit(solution)/shard_map/dot_general | solution.py:207
  222.8 12.4 %convolution_convert_fusion = bf16[1024,2048]{1,0:T(8,128)(2,1)} fusion(bf16[2048,2112]{0,1:T(8,128)(2,1)} %all-gather.4.cloned.1.call-done, f32[1024,704]{0,1:T(8,128)} %fusion.8, bf16[1024,2048]{1,0:T(8,128)(2,1)} %get-tuple-element.79, f32[2048]{0:T(1024)S(1)} %copy-done.31, f32[1024]{0:T(1024)S(1)} %add_rsqrt_fusion), kind=kOutput, calls=%fused_computation.12 | convolution fusion | flops 5920391168 | bytes 17051648 | tf_op jit(solution)/shard_map/dot_general | solution.py:210
  235.3 38.4 %reduce-scatter.2.cloned.1.call-done = bf16[1024,256]{1,0:T(8,128)(2,1)} async-done(((bf16[1024,2048]{1,0:T(8,128)(2,1)}), bf16[1024,256]{1,0:T(8,128)(2,1)}) %reduce-scatter.2.cloned.1.call-update) | async-done | bytes 524304 | tf_op jit(solution)/shard_map/reduce_scatter | solution.py:212
  273.6 2.2 add_convert_fusion.1
  (121 shorter events, 22.6 us)
Async XLA Ops:
  7.4 123.9 %copy-start = (bf16[512,2048]{1,0:T(8,128)(2,1)S(1)}, bf16[512,2048]{1,0:T(8,128)(2,1)}, u32[]{:S(2)}) copy-start(bf16[512,2048]{1,0:T(8,128)(2,1)} %param.31) | copy-start | bytes 6291460
  7.4 17.0 %copy-start.33 = (u32[128]{0:T(128)S(1)}, u32[128]{0:T(128)}, u32[]{:S(2)}) copy-start(u32[128]{0:T(128)} %constant.76) | copy-start | bytes 1540
  7.4 199.9 %all-reduce.3.cloned.1.call-start = ((), (), s32[]{:S(2)}) async-start(), calls=%async_computation.1 | async-start | bytes 8388608 | tf_op jit(solution)/shard_map/psum | solution.py:198
  9.0 52.9 %collective-permute-start.1 = (bf16[3,256]{0,1:T(8,128)(2,1)}, bf16[3,256]{0,1:T(8,128)(2,1)}, u32[]{:S(2)}, u32[]{:S(2)}) collective-permute-start(bf16[3,256]{0,1:T(8,128)(2,1)} %bitcast.4), channel_id=1, source_target_pairs={{0,8},{8,16},{16,24},{24,32},{32,40},{40,48},{48,56},{56,64},{64,7... | collective-permute-start | bytes 4616 | tf_op jit(solution)/shard_map/ppermute | solution.py:27
  14.7 56.8 %collective-permute-start = (bf16[3,512]{0,1:T(8,128)(2,1)}, bf16[3,512]{0,1:T(8,128)(2,1)S(1)}, u32[]{:S(2)}, u32[]{:S(2)}) collective-permute-start(bf16[3,512]{0,1:T(8,128)(2,1)} %copy.50), channel_id=1, source_target_pairs={{0,8},{8,16},{16,24},{24,32},{32,40},{40,48},{48,56},{56,64},{64,7... | collective-permute-start | bytes 9224 | tf_op jit(solution)/shard_map/ppermute | solution.py:27
  24.3 1.3 copy-start.19
  47.8 5.6 %copy-start.30 = (f32[8]{0:T(128)S(1)}, f32[8]{0:T(128)}, u32[]{:S(2)}) copy-start(f32[8]{0:T(128)} %param.29) | copy-start | bytes 100
  73.3 2.2 copy-start.2
  75.5 0.8 copy-start.15
  75.5 1.0 copy-start.7
  75.8 2.5 copy-start.4
  78.3 32.0 %copy-start.21 = (f32[8]{0:T(128)S(1)}, f32[8]{0:T(128)}, u32[]{:S(2)}) copy-start(f32[8]{0:T(128)} %get-tuple-element.108) | copy-start | bytes 100
  78.3 32.0 %copy-start.22 = (f32[8]{0:T(128)S(1)}, f32[8]{0:T(128)}, u32[]{:S(2)}) copy-start(f32[8]{0:T(128)} %get-tuple-element.109) | copy-start | bytes 100
  78.3 32.0 %copy-start.23 = (f32[8]{0:T(128)S(1)}, f32[8]{0:T(128)}, u32[]{:S(2)}) copy-start(f32[8]{0:T(128)} %get-tuple-element.110) | copy-start | bytes 100
  78.3 32.0 %copy-start.24 = (f32[8]{0:T(128)S(1)}, f32[8]{0:T(128)}, u32[]{:S(2)}) copy-start(f32[8]{0:T(128)} %get-tuple-element.111) | copy-start | bytes 100
  97.3 26.4 %copy-start.6 = (bf16[1024,1,1,128]{3,0,2,1:T(8,128)(2,1)S(1)}, bf16[1024,1,1,128]{3,0,2,1:T(8,128)(2,1)}, u32[]{:S(2)}) copy-start(bf16[1024,1,1,128]{3,0,2,1:T(8,128)(2,1)} %copy.54) | copy-start | bytes 786436
  97.3 26.3 %copy-start.8 = (bf16[8,1,8,64,128]{4,3,2,1,0:T(8,128)(2,1)S(1)}, bf16[8,1,8,64,128]{4,3,2,1,0:T(8,128)(2,1)}, u32[]{:S(2)}) copy-start(bf16[8,1,8,64,128]{4,3,2,1,0:T(8,128)(2,1)} %get-tuple-element.33) | copy-start | bytes 3145732
  110.5 13.6 %copy-start.5 = (bf16[64,8,8,128]{3,2,1,0:T(8,128)(2,1)S(1)}, bf16[64,8,8,128]{3,2,1,0:T(8,128)(2,1)}, u32[]{:S(2)}) copy-start(bf16[64,8,8,128]{3,2,1,0:T(8,128)(2,1)} %copy-done.4) | copy-start | bytes 3145732
  110.5 13.6 %copy-start.9 = (f32[8,128,128]{2,1,0:T(8,128)S(1)}, f32[8,128,128]{2,1,0:T(8,128)}, u32[]{:S(2)}) copy-start(f32[8,128,128]{2,1,0:T(8,128)} %fusion.108) | copy-start | bytes 1572868
  110.5 13.6 %copy-start.16 = (f32[8,8,128]{2,1,0:T(8,128)S(1)}, f32[8,8,128]{2,1,0:T(8,128)}, u32[]{:S(2)}) copy-start(f32[8,8,128]{2,1,0:T(8,128)} %copy.57) | copy-start | bytes 98308
  110.5 13.6 %copy-start.17 = (f32[8,8,128]{2,1,0:T(8,128)S(1)}, f32[8,8,128]{2,1,0:T(8,128)}, u32[]{:S(2)}) copy-start(f32[8,8,128]{2,1,0:T(8,128)} %get-tuple-element.92) | copy-start | bytes 98308
  110.5 13.6 %copy-start.18 = (pred[128,128]{1,0:T(8,128)(4,1)S(1)}, pred[128,128]{1,0:T(8,128)(4,1)}, u32[]{:S(2)}) copy-start(pred[128,128]{1,0:T(8,128)(4,1)} %iota_compare_fusion) | copy-start | bytes 49156
  124.1 1.7 copy-start.13
  124.1 1.7 copy-start.14
  124.2 1.7 copy-start.25
  124.2 1.7 copy-start.26
  124.2 1.7 copy-start.27
  124.2 1.7 copy-start.28
  124.2 1.7 copy-start.29
  126.7 1.7 copy-start.3
  126.7 1.7 copy-start.20
  128.4 2.9 %copy-start.32 = (f32[512]{0:T(512)S(1)}, f32[512]{0:T(512)}, u32[]{:S(2)}) copy-start(f32[512]{0:T(512)} %param.30) | copy-start | bytes 6148
  135.8 0.9 copy-start.10
  135.8 1.0 copy-start.11
  135.8 1.1 copy-start.12
  135.9 79.1 %all-gather.4.cloned.1.call-start = ((), (), s32[]{:S(2)}) async-start(), calls=%async_computation.2 | async-start | bytes 9191424 | tf_op jit(solution)/shard_map/all_gather | solution.py:16
  137.8 77.1 %copy-start.31 = (f32[2048]{0:T(1024)S(1)}, f32[2048]{0:T(1024)}, u32[]{:S(2)}) copy-start(f32[2048]{0:T(1024)} %param.32) | copy-start | bytes 24580
  137.8 135.8 %reduce-scatter.2.cloned.1.call-start = ((), (), s32[]{:S(2)}) async-start(), calls=%async_computation.3 | async-start | bytes 4718592 | tf_op jit(solution)/shard_map/reduce_scatter | solution.py:212
  235.2 40.6 %copy-start.1 = (bf16[512,2048]{1,0:T(8,128)(2,1)S(1)}, bf16[512,2048]{1,0:T(8,128)(2,1)}, u32[]{:S(2)}) copy-start(bf16[512,2048]{1,0:T(8,128)(2,1)} %param.31) | copy-start | bytes 6291460
Sparse Core Ops, SparseCore 0:
  136.0 71.1 all-reduce.2
  235.4 38.2 reduce-scatter.1
Sparse Core Ops, SparseCore 1:
  138.5 76.4 all-gather.3
where the time goes:
time: 284 us; the launch traced here: 283 us
  waiting for transfers between devices  108 us (38%)
  blocking collectives  46 us (16%)
  other arithmetic  43.5 us (15%)
  matrix products  31.6 us (11%)
  local copies, waits for them, and re-layouts  30.9 us (11%)
  between operations  16 us (6%)
  starting transfers between devices  7.38 us (3%)
    psum x1, waiting for transfers between devices, shards(): mixer_out = lax.psum(rounded.astype(jnp.bfloat16), 'tp').astype(jnp.float32)  69.1 us
    reduce_scatter x1, waiting for transfers between devices, shards(): lax.psum_scatter(down_rounded.astype(jnp.bfloat16), 'tp', scatter_dimensi...  38.4 us
    all_gather x3, blocking collectives, entering_2(): lax.all_gather(part.astype(kind), axis)  35.3 us
    dot_general x1, matrix products, shards(): down_terms = jnp.dot(hidden, whole_down, preferred_element_type=jnp.float32)  12.4 us
    unnamed x1, blocking collectives  10.7 us
    unnamed x75, local copies, waits for them, and re-layouts  8.9 us
    add x8, other arithmetic, carry_step(): carry_state * jnp.exp(block_end)[:, :, None, None] + block_added  8.32 us
    dot_general x1, matrix products, shards(): gate_pre = jnp.dot(normed, whole_gate, preferred_element_type=jnp.float32)  7.9 us
  transfers between devices with their start and end apart: 5, of which 3 were waited for; matrix products, arithmetic and copies ran while one was open for 15% of the time, Pallas kernels for 0%

commit v1 on v0

--- a/solution.py
+++ b/solution.py
@@ -8,6 +8,11 @@
 BLOCK_POSITIONS = 128
 SP = ("sp_0", "sp_1")
 EPS = 1e-06
+
+
+def summed_here(value, name):
+    parts = lax.all_gather(value, name)
+    return jnp.sum(parts, axis=0)
 
 
 def rows_first(arrays, axis, dims):
@@ -195,7 +200,7 @@
     rounded = lax.optimization_barrier(partial_sum.astype(jnp.bfloat16)).astype(jnp.float32)
     col_count = D // lax.axis_size("tp")
     offset = lax.axis_index("tp") * col_count
-    mixer_out = lax.psum(rounded.astype(jnp.bfloat16), "tp").astype(jnp.float32)
+    mixer_out = summed_here(rounded.astype(jnp.bfloat16), "tp").astype(jnp.float32)
     residual_whole = (arriving_hidden_sum.astype(jnp.float32) + mixer_out).astype(jnp.bfloat16)
     squares = residual_whole.astype(jnp.float32)
     normed = (

time: 284 us -> 460 us (1.62)
  waiting for transfers between devices: 108 us -> 249 us
  other arithmetic: 43.5 us -> 78.2 us
    all_gather x0 -> x1, waiting for transfers between devices: none -> 152 us  [summed_here(): parts = lax.all_gather(value, name)]
    psum x1 -> x0, waiting for transfers between devices: 69.1 us -> none  [shards(): mixer_out = lax.psum(rounded.astype(jnp.bfloat16), 'tp').astype(jnp.float32)]
    all_gather x1, waiting for transfers between devices: 0.16 us -> 60.1 us  [rows_first(): out, at, outs = (lax.all_gather(both, axis, axis=0, tiled=True), 0, [])]
    another operation x1, other arithmetic: 1.18 us -> 23.3 us  [shards(): cum_log = jnp.cumsum(fading_log_factor, axis=1)]
    reduce_sum x0 -> x1, other arithmetic: none -> 14.2 us  [summed_here(): return jnp.sum(parts, axis=0)]
    unnamed x75 -> x79, local copies, waits for them, and re-layouts: 8.9 us -> 9.54 us
  transfers between devices with their start and end apart: 5 -> 5, of which waited for: 3 -> 3; matrix products, arithmetic and copies ran while one was open for 15% -> 17% of each run, Pallas kernels for 0% -> 0%
where the time goes in v1:
time: 460 us; the launch traced here: 459 us
  waiting for transfers between devices  249 us (54%)
  other arithmetic  78.2 us (17%)
  blocking collectives  45.4 us (10%)
  local copies, waits for them, and re-layouts  31.8 us (7%)
  matrix products  31.7 us (7%)
  between operations  14.3 us (3%)
  starting transfers between devices  8.01 us (2%)
    all_gather x1, waiting for transfers between devices, summed_here(): parts = lax.all_gather(value, name)  152 us
    all_gather x1, waiting for transfers between devices, rows_first(): out, at, outs = (lax.all_gather(both, axis, axis=0, tiled=True), 0, [])  60.1 us
    reduce_scatter x1, waiting for transfers between devices, shards(): lax.psum_scatter(down_rounded.astype(jnp.bfloat16), 'tp', scatter_dimensi...  37.2 us
    all_gather x3, blocking collectives, entering_2(): lax.all_gather(part.astype(kind), axis)  35.3 us
    another operation x1, other arithmetic, shards(): cum_log = jnp.cumsum(fading_log_factor, axis=1)  23.3 us
    reduce_sum x1, other arithmetic, summed_here(): return jnp.sum(parts, axis=0)  14.2 us
    dot_general x1, matrix products, shards(): down_terms = jnp.dot(hidden, whole_down, preferred_element_type=jnp.float32)  12.5 us
    unnamed x1, blocking collectives  10.1 us
  transfers between devices with their start and end apart: 5, of which 3 were waited for; matrix products, arithmetic and copies ran while one was open for 17% of the time, Pallas kernels for 0%

profile of v1, /device:TPU:0, one launch (start us, length us, event | category | flops | bytes accessed | tf_op | source)
XLA Modules:
  0.0 458.7 jit_solution(16379918566008575677)
XLA Ops:
  6.6 0.8 slice.127
  8.2 3.6 collective-permute-start
  13.3 4.1 collective-permute-start.1
  18.0 1.5 fusion.102
  19.7 23.3 %fusion.107 = f32[8,128,8]{2,0,1:T(8,128)S(1)} fusion(f32[8,128,8]{2,0,1:T(8,128)S(1)} %copy.56), kind=kOutput, calls=%fused_computation.174 | output fusion | flops 1040384 | bytes 65536 | tf_op jit(solution)/shard_map/jit(cumsum)/reduce_window_sum | solution.py:131
  46.1 10.1 %all-reduce = bf16[32]{0:T(256)(128)(2,1)S(1)} all-reduce(bf16[32]{0:T(256)(128)(2,1)S(1)} %dynamic-update-slice), channel_id=2, replica_groups=mesh['sp_0'=4,'sp_1'=4,'tp'=8] {'sp_1'}, use_global_device_ids=true, to_apply=%add | all-reduce | flops 32 | bytes 128
  56.3 9.3 %all_gather.28 = bf16[4,1,8]{2,1,0:T(2,128)(2,1)S(1)} all-gather(bf16[1,1,8]{2,1,0:T(2,128)(2,1)S(1)} %get-tuple-element.82), channel_id=1, replica_groups=mesh['sp_0'=4,'sp_1'=4,'tp'=8] {'sp_0'}, dimensions={0}, use_global_device_ids=true | all-gather | bytes 80 | tf_op jit(solution)/shard_map/all_gather | solution.py:47
  66.1 1.2 fusion.105
  68.6 2.3 copy.51
  71.0 2.0 copy.53
  73.0 1.8 copy.61
  75.6 1.8 copy.65
  78.2 1.5 copy.69
  79.7 1.3 mul.381
  81.0 1.3 mul.382
  82.4 1.3 maximum_convert_fusion.1
  83.7 1.8 multiply_convert_fusion.7
  86.3 1.8 copy.55
  88.1 1.8 copy.54
  89.9 2.1 fusion.108
  92.0 1.8 maximum_convert_fusion
  93.8 2.2 fusion.116
  97.1 1.8 convolution_bitcast_fusion
  98.9 19.1 %while.13 = (s32[]{:T(128)}, f32[1,8,64,128]{3,2,1,0:T(8,128)S(1)}, bf16[8,1,8,64,128]{4,3,2,1,0:T(8,128)(2,1)}, f32[8,1,8]{2,1,0:T(1,128)}, f32[8,1,8,64,128]{4,3,2,1,0:T(8,128)}, /*index=5*/s32[]{:T(128)}, s32[]{:T(128)}) while((s32[]{:T(128)}, f32[1,8,64,128]{3,2,1,0:T(8,128)S(1)}, bf16[8,1,8,64,128]{4,3,2,1,0:T(8,128)(2,1)}, ...), condition=%wide.region_2.3_spmd.clone, body=%wide.region_1.2_spmd.clone.sunk | while | flops 262147 | bytes 1180352 | solution.py:164
  100.2 1.0 bitcast_add_fusion.3
  102.6 1.0 bitcast_add_fusion.3
  105.0 1.0 bitcast_add_fusion.3
  107.4 1.0 bitcast_add_fusion.3
  109.8 1.0 bitcast_add_fusion.3
  112.2 1.0 bitcast_add_fusion.3
  114.5 1.0 bitcast_add_fusion.3
  116.9 1.0 bitcast_add_fusion.3
  118.0 12.9 %all-gather.1 = bf16[4,8,64,128]{3,2,1,0:T(8,128)(2,1)S(1)} all-gather(bf16[1,8,64,128]{3,2,1,0:T(8,128)(2,1)S(1)} %convert_element_type.349), channel_id=3, replica_groups=mesh['sp_0'=4,'sp_1'=4,'tp'=8] {'sp_1'}, dimensions={0}, use_global_device_ids=true | all-gather | bytes 655360 | tf_op jit(solution)/shard_map/all_gather | solution.py:47
  131.2 13.1 %all_gather.31 = bf16[4,1,8,64,128]{4,3,2,1,0:T(8,128)(2,1)S(1)} all-gather(bf16[1,1,8,64,128]{4,3,2,1,0:T(8,128)(2,1)S(1)} %fusion.66), channel_id=1, replica_groups=mesh['sp_0'=4,'sp_1'=4,'tp'=8] {'sp_0'}, dimensions={0}, use_global_device_ids=true | all-gather | bytes 655360 | tf_op jit(solution)/shard_map/all_gather | solution.py:47
  144.9 1.6 fusion.10
  147.4 1.2 copy.68
  149.1 2.9 multiply_reduce_fusion
  152.0 4.5 convolution_convert_fusion.1
  156.5 0.8 copy-done.11
  157.5 0.8 pad_maximum_fusion
  158.7 151.9 %all-gather.8.cloned.1.call-done = bf16[8192,2048]{1,0:T(8,128)(2,1)} async-done(((bf16[1024,2048]{1,0:T(8,128)(2,1)}), bf16[8192,2048]{1,0:T(8,128)(2,1)}) %all-gather.8.cloned.1.call-update) | async-done | bytes 33554448 | tf_op jit(solution)/shard_map/all_gather | solution.py:14
  310.5 14.2 %reduce_sum.41 = bf16[1024,2048]{1,0:T(8,128)(2,1)} reduce(bf16[8,1024,2048]{2,1,0:T(8,128)(2,1)} %bitcast.153, bf16[]{:T(256)} %constant.68.clone.1), dimensions={0}, to_apply=%region_6.7 | reduce | flops 14680064 | bytes 37748736 | tf_op jit(solution)/shard_map/reduce_sum | solution.py:15
  324.7 7.5 %fusion.2 = (f32[1024]{0:T(1024)S(1)}, bf16[1024,2048]{1,0:T(8,128)(2,1)}) fusion(bf16[1024,2048]{1,0:T(8,128)(2,1)} %reduce_sum.41, bf16[1024,2048]{1,0:T(8,128)(2,1)} %param.19), kind=kLoop, calls=%fused_computation.7 | loop fusion | flops 14679040 | bytes 12587008 | tf_op jit(solution)/shard_map/reduce_sum | solution.py:208
  332.2 60.1 %all-gather.6.cloned.1.call-done = bf16[2048,2112]{0,1:T(8,128)(2,1)} async-done(((bf16[128,2112]{0,1:T(8,128)(2,1)}), bf16[2048,2112]{0,1:T(8,128)(2,1)}) %all-gather.6.cloned.1.call-update) | async-done | bytes 8650768 | tf_op jit(solution)/shard_map/all_gather | solution.py:21
  392.3 8.0 %fusion.8 = f32[1024,704]{0,1:T(8,128)} fusion(bf16[2048,2112]{0,1:T(8,128)(2,1)} %all-gather.6.cloned.1.call-done, bf16[1024,2048]{1,0:T(8,128)(2,1)} %get-tuple-element.79, f32[2048]{0:T(1024)S(1)} %copy-done.33, f32[1024]{0:T(1024)S(1)} %add_rsqrt_fusion), kind=kOutput, calls=%fused_computation.17 | convolution fusion | flops 2961178624 | bytes 9973760 | tf_op jit(solution)/shard_map/dot_general | solution.py:212
  400.3 12.5 %convolution_convert_fusion = bf16[1024,2048]{1,0:T(8,128)(2,1)} fusion(bf16[2048,2112]{0,1:T(8,128)(2,1)} %all-gather.6.cloned.1.call-done, f32[1024,704]{0,1:T(8,128)} %fusion.8, bf16[1024,2048]{1,0:T(8,128)(2,1)} %get-tuple-element.79, f32[2048]{0:T(1024)S(1)} %copy-done.33, f32[1024]{0:T(1024)S(1)} %add_rsqrt_fusion), kind=kOutput, calls=%fused_computation.12 | convolution fusion | flops 5920391168 | bytes 17051648 | tf_op jit(solution)/shard_map/dot_general | solution.py:215
  412.8 37.2 %reduce-scatter.2.cloned.1.call-done = bf16[1024,256]{1,0:T(8,128)(2,1)} async-done(((bf16[1024,2048]{1,0:T(8,128)(2,1)}), bf16[1024,256]{1,0:T(8,128)(2,1)}) %reduce-scatter.2.cloned.1.call-update) | async-done | bytes 524304 | tf_op jit(solution)/shard_map/reduce_scatter | solution.py:217
  450.0 2.2 add_convert_fusion.1
  (126 shorter events, 24.0 us)
Async XLA Ops:
  6.5 145.4 %copy-start = (bf16[512,2048]{1,0:T(8,128)(2,1)S(1)}, bf16[512,2048]{1,0:T(8,128)(2,1)}, u32[]{:S(2)}) copy-start(bf16[512,2048]{1,0:T(8,128)(2,1)} %param.31) | copy-start | bytes 6291460
  6.5 38.0 %copy-start.35 = (u32[128]{0:T(128)S(1)}, u32[128]{0:T(128)}, u32[]{:S(2)}) copy-start(u32[128]{0:T(128)} %constant.78) | copy-start | bytes 1540
  6.5 37.4 %copy-start.20 = (bf16[4,512]{1,0:T(4,128)(2,1)S(1)}, bf16[4,512]{1,0:T(4,128)(2,1)}, u32[]{:S(2)}) copy-start(bf16[4,512]{1,0:T(4,128)(2,1)} %param.25) | copy-start | bytes 12292
  6.5 37.4 %copy-start.32 = (bf16[4,1,2,128]{3,2,1,0:T(2,128)(2,1)S(1)}, bf16[4,1,2,128]{3,2,1,0:T(2,128)(2,1)}, u32[]{:S(2)}) copy-start(bf16[4,1,2,128]{3,2,1,0:T(2,128)(2,1)} %param.26) | copy-start | bytes 6148
  6.5 304.0 %all-gather.8.cloned.1.call-start = ((), (), s32[]{:S(2)}) async-start(), calls=%async_computation.3 | async-start | bytes 37748736 | tf_op jit(solution)/shard_map/all_gather | solution.py:14
  8.2 83.8 %collective-permute-start = (bf16[3,512]{0,1:T(8,128)(2,1)}, bf16[3,512]{0,1:T(8,128)(2,1)S(1)}, u32[]{:S(2)}, u32[]{:S(2)}) collective-permute-start(bf16[3,512]{0,1:T(8,128)(2,1)} %copy.50), channel_id=1, source_target_pairs={{0,8},{8,16},{16,24},{24,32},{32,40},{40,48},{48,56},{56,64},{64,7... | collective-permute-start | bytes 9224 | tf_op jit(solution)/shard_map/ppermute | solution.py:32
  13.3 69.1 %collective-permute-start.1 = (bf16[3,256]{0,1:T(8,128)(2,1)}, bf16[3,256]{0,1:T(8,128)(2,1)}, u32[]{:S(2)}, u32[]{:S(2)}) collective-permute-start(bf16[3,256]{0,1:T(8,128)(2,1)} %bitcast.4), channel_id=1, source_target_pairs={{0,8},{8,16},{16,24},{24,32},{32,40},{40,48},{48,56},{56,64},{64,7... | collective-permute-start | bytes 4616 | tf_op jit(solution)/shard_map/ppermute | solution.py:32
  43.1 0.6 copy-start.21
  68.6 8.8 %copy-start.8 = (f32[8,128,8]{2,0,1:T(8,128)S(1)}, f32[8,128,8]{2,0,1:T(8,128)}, u32[]{:S(2)}) copy-start(f32[8,128,8]{2,0,1:T(8,128)} %get-tuple-element.88) | copy-start | bytes 98308
  93.8 2.2 copy-start.2
  96.1 0.8 copy-start.16
  96.1 1.0 copy-start.7
  96.4 2.5 copy-start.4
  98.8 32.1 %copy-start.23 = (f32[8]{0:T(128)S(1)}, f32[8]{0:T(128)}, u32[]{:S(2)}) copy-start(f32[8]{0:T(128)} %get-tuple-element.108) | copy-start | bytes 100
  98.8 32.1 %copy-start.24 = (f32[8]{0:T(128)S(1)}, f32[8]{0:T(128)}, u32[]{:S(2)}) copy-start(f32[8]{0:T(128)} %get-tuple-element.109) | copy-start | bytes 100
  98.8 32.1 %copy-start.25 = (f32[8]{0:T(128)S(1)}, f32[8]{0:T(128)}, u32[]{:S(2)}) copy-start(f32[8]{0:T(128)} %get-tuple-element.110) | copy-start | bytes 100
  98.8 32.1 %copy-start.26 = (f32[8]{0:T(128)S(1)}, f32[8]{0:T(128)}, u32[]{:S(2)}) copy-start(f32[8]{0:T(128)} %get-tuple-element.111) | copy-start | bytes 100
  118.0 26.4 %copy-start.6 = (bf16[1024,1,1,128]{3,0,2,1:T(8,128)(2,1)S(1)}, bf16[1024,1,1,128]{3,0,2,1:T(8,128)(2,1)}, u32[]{:S(2)}) copy-start(bf16[1024,1,1,128]{3,0,2,1:T(8,128)(2,1)} %copy.54) | copy-start | bytes 786436
  118.0 26.3 %copy-start.9 = (bf16[8,1,8,64,128]{4,3,2,1,0:T(8,128)(2,1)S(1)}, bf16[8,1,8,64,128]{4,3,2,1,0:T(8,128)(2,1)}, u32[]{:S(2)}) copy-start(bf16[8,1,8,64,128]{4,3,2,1,0:T(8,128)(2,1)} %get-tuple-element.33) | copy-start | bytes 3145732
  131.2 13.6 %copy-start.5 = (bf16[64,8,8,128]{3,2,1,0:T(8,128)(2,1)S(1)}, bf16[64,8,8,128]{3,2,1,0:T(8,128)(2,1)}, u32[]{:S(2)}) copy-start(bf16[64,8,8,128]{3,2,1,0:T(8,128)(2,1)} %copy-done.4) | copy-start | bytes 3145732
  131.2 13.6 %copy-start.10 = (f32[8,128,128]{2,1,0:T(8,128)S(1)}, f32[8,128,128]{2,1,0:T(8,128)}, u32[]{:S(2)}) copy-start(f32[8,128,128]{2,1,0:T(8,128)} %fusion.108) | copy-start | bytes 1572868
  131.2 13.6 %copy-start.17 = (f32[8,8,128]{2,1,0:T(8,128)S(1)}, f32[8,8,128]{2,1,0:T(8,128)}, u32[]{:S(2)}) copy-start(f32[8,8,128]{2,1,0:T(8,128)} %copy.57) | copy-start | bytes 98308
  131.2 13.6 %copy-start.18 = (f32[8,8,128]{2,1,0:T(8,128)S(1)}, f32[8,8,128]{2,1,0:T(8,128)}, u32[]{:S(2)}) copy-start(f32[8,8,128]{2,1,0:T(8,128)} %get-tuple-element.92) | copy-start | bytes 98308
  131.2 13.6 %copy-start.19 = (pred[128,128]{1,0:T(8,128)(4,1)S(1)}, pred[128,128]{1,0:T(8,128)(4,1)}, u32[]{:S(2)}) copy-start(pred[128,128]{1,0:T(8,128)(4,1)} %iota_compare_fusion) | copy-start | bytes 49156
  144.8 1.7 copy-start.14
  144.8 1.7 copy-start.15
  144.8 1.7 copy-start.27
  144.8 1.7 copy-start.28
  144.8 1.7 copy-start.29
  144.9 1.7 copy-start.30
  144.9 1.7 copy-start.31
  147.4 1.7 copy-start.3
  147.4 1.7 copy-start.22
  149.1 2.9 copy-start.34
  156.4 0.9 copy-start.11
  156.5 1.0 copy-start.12
  156.5 1.1 copy-start.13
  156.5 235.9 %all-gather.6.cloned.1.call-start = ((), (), s32[]{:S(2)}) async-start(), calls=%async_computation.1 | async-start | bytes 9191424 | tf_op jit(solution)/shard_map/all_gather | solution.py:21
  158.4 291.6 %reduce-scatter.2.cloned.1.call-start = ((), (), s32[]{:S(2)}) async-start(), calls=%async_computation.2 | async-start | bytes 4718592 | tf_op jit(solution)/shard_map/reduce_scatter | solution.py:217
  324.7 67.6 %copy-start.33 = (f32[2048]{0:T(1024)S(1)}, f32[2048]{0:T(1024)}, u32[]{:S(2)}) copy-start(f32[2048]{0:T(1024)} %param.32) | copy-start | bytes 24580
  412.7 39.4 %copy-start.1 = (bf16[512,2048]{1,0:T(8,128)(2,1)S(1)}, bf16[512,2048]{1,0:T(8,128)(2,1)}, u32[]{:S(2)}) copy-start(bf16[512,2048]{1,0:T(8,128)(2,1)} %param.31) | copy-start | bytes 6291460
Sparse Core Ops, SparseCore 0:
  156.6 153.8 all-gather.7
  312.7 79.6 all-gather.5
  412.9 37.0 reduce-scatter.1
